TPU v7x, 32 devices: a whole 2x2x4 slice. The times are simulated.
32 devices in a mesh: fs: 8 (over z, x), tp: 4 (over y, core).
Axes of the slice: x: 2, y: 2, z: 4, core: 2. Of those that a mesh axis runs over, the one named last changes fastest.
Arguments:
- q_latent: bfloat16 [6144, 512], P('fs'), may hold values from -6 to 6
- q_grad: bfloat16 [6144, 3072], P('fs', 'tp'), may hold values from -6 to 6
- uq_master: float32 [512, 3072], P('fs', 'tp'), may hold values from -6 to 6
- uq_basis: bfloat16 [512, 256], P('fs'), may hold values from -4 to 4
- uq_first: float32 [256, 3072], P('fs', 'tp'), may hold values from -3 to 3
- uq_second: float32 [256, 3072], P('fs', 'tp'), may hold values from 0.1 to 1
- kv_latent: bfloat16 [6144, 512], P('fs'), may hold values from -6 to 6
- k_grad: bfloat16 [6144, 2048], P('fs', 'tp'), may hold values from -6 to 6
- uk_master: float32 [512, 2048], P('fs', 'tp'), may hold values from -6 to 6
- uk_basis: bfloat16 [512, 256], P('fs'), may hold values from -4 to 4
- uk_first: float32 [256, 2048], P('fs', 'tp'), may hold values from -3 to 3
- uk_second: float32 [256, 2048], P('fs', 'tp'), may hold values from 0.1 to 1
Outputs:
- uq_first_new: float32 [256, 3072], P('fs', 'tp')
- uq_second_new: float32 [256, 3072], P('fs', 'tp')
- uq_step: float32 [512, 3072], P('fs', 'tp')
- uq_copy: bfloat16 [512, 3072], P(None, 'tp')
- uk_first_new: float32 [256, 2048], P('fs', 'tp')
- uk_second_new: float32 [256, 2048], P('fs', 'tp')
- uk_step: float32 [512, 2048], P('fs', 'tp')
- uk_copy: bfloat16 [512, 2048], P(None, 'tp')
All inputs are finite; a program needn't handle non-finite values.
Results may differ from a plain program's by a relative error of at most 0.0071.
Values may be sent and summed in bfloat16 or wider, within the bound.
A program may use at most 64 MiB of HBM per device.

v0:
```python
import jax
import jax.numpy as jnp
from jax import lax
from jax.sharding import PartitionSpec as P

first_decay = 0.8
second_decay = 0.9
step_size = 0.5
mean_guard = 1e-06
root_guard = 1e-08


def across_tokens(left, right):
    return lax.dot_general(
        left, right, (((0,), (0,)), ((), ())), preferred_element_type=jnp.float32
    )


def across_latent(left, right):
    return lax.dot_general(
        left,
        right,
        (((0,), (0,)), ((), ())),
        precision=lax.Precision.HIGHEST,
        preferred_element_type=jnp.float32,
    )


def moment_update(scaled, first_old, second_old):
    first_new = first_decay * first_old + (1.0 - first_decay) * scaled
    second_new = second_decay * second_old + (1.0 - second_decay) * scaled * scaled
    heading = (first_new / (jnp.sqrt(second_new) + root_guard)).astype(jnp.bfloat16)
    return (first_new, second_new, heading)


def body(
    q_latent,
    q_grad,
    uq_master,
    uq_basis,
    uq_first,
    uq_second,
    kv_latent,
    k_grad,
    uk_master,
    uk_basis,
    uk_first,
    uk_second,
):
    q_width = q_grad.shape[1]
    q_whole, k_whole = (
        lax.all_gather(uq_basis, "fs", axis=0, tiled=True),
        lax.all_gather(uk_basis, "fs", axis=0, tiled=True),
    )
    q_factor = q_whole.astype(jnp.float32)
    k_factor = k_whole.astype(jnp.float32)
    q_partial = across_tokens(q_latent, q_grad)
    k_partial = across_tokens(kv_latent, k_grad)
    projected = lax.psum_scatter(
        jnp.concatenate(
            [across_latent(q_factor, q_partial), across_latent(k_factor, k_partial)], axis=1
        ),
        "fs",
        scatter_dimension=0,
        tiled=True,
    )
    squares_sum = lax.psum(jnp.sum(projected * projected), ("fs", "tp"))
    entry_count = (
        projected.shape[0] * projected.shape[1] * lax.axis_size("fs") * lax.axis_size("tp")
    )
    root_mean = jnp.sqrt(squares_sum / entry_count + mean_guard)
    scaled = projected / root_mean
    uq_first_new, uq_second_new, q_heading = moment_update(scaled[:, :q_width], uq_first, uq_second)
    uk_first_new, uk_second_new, k_heading = moment_update(scaled[:, q_width:], uk_first, uk_second)
    q_dir, k_dir = (
        lax.all_gather(q_heading, "fs", axis=0, tiled=True),
        lax.all_gather(k_heading, "fs", axis=0, tiled=True),
    )
    uq_step = jnp.dot(uq_basis, q_dir, preferred_element_type=jnp.float32)
    uk_step = jnp.dot(uk_basis, k_dir, preferred_element_type=jnp.float32)
    q_fresh = (uq_master - step_size * uq_step).astype(jnp.bfloat16)
    k_fresh = (uk_master - step_size * uk_step).astype(jnp.bfloat16)
    uq_copy, uk_copy = (
        lax.all_gather(q_fresh, "fs", axis=0, tiled=True),
        lax.all_gather(k_fresh, "fs", axis=0, tiled=True),
    )
    return (
        uq_first_new,
        uq_second_new,
        uq_step,
        uq_copy,
        uk_first_new,
        uk_second_new,
        uk_step,
        uk_copy,
    )


def solution(mesh):
    return jax.shard_map(
        body,
        mesh=mesh,
        in_specs=(
            P("fs", None),
            P("fs", "tp"),
            P("fs", "tp"),
            P("fs", None),
            P("fs", "tp"),
            P("fs", "tp"),
            P("fs", None),
            P("fs", "tp"),
            P("fs", "tp"),
            P("fs", None),
            P("fs", "tp"),
            P("fs", "tp"),
        ),
        out_specs=(
            P("fs", "tp"),
            P("fs", "tp"),
            P("fs", "tp"),
            P(None, "tp"),
            P("fs", "tp"),
            P("fs", "tp"),
            P("fs", "tp"),
            P(None, "tp"),
        ),
        check_vma=False,
    )
```

profile of v0, /device:TPU:0, one launch (start us, length us, event | category | flops | bytes accessed | tf_op | source)
XLA Modules:
  0.0 323.5 jit_solution(11529704585300049106)
XLA Ops:
  7.2 0.0 copy-start
  7.2 0.0 reduce-scatter.4.cloned.1.call-start
  7.2 32.9 %all_gather.18 = bf16[512,256]{1,0:T(8,128)(2,1)S(1)} all-gather(bf16[64,256]{1,0:T(8,128)(2,1)} %param.15), channel_id=1, replica_groups=mesh['fs'=8,'tp'=4] {'fs'}, dimensions={0}, use_global_device_ids=true | all-gather | bytes 294912 | tf_op jit(solution)/shard_map/all_gather | solution.py:52
  40.2 30.9 %all_gather.19 = bf16[512,256]{1,0:T(8,128)(2,1)S(1)} all-gather(bf16[64,256]{1,0:T(8,128)(2,1)} %param.21), channel_id=1, replica_groups=mesh['fs'=8,'tp'=4] {'fs'}, dimensions={0}, use_global_device_ids=true | all-gather | bytes 294912 | tf_op jit(solution)/shard_map/all_gather | solution.py:53
  71.1 1.9 fusion.4
  73.1 0.0 copy-start.1
  73.1 0.0 copy-start.2
  73.1 1.4 convolution_bitcast_fusion
  74.5 0.6 fusion.5
  75.1 1.0 convolution_bitcast_fusion.1
  76.1 0.1 pad_maximum_fusion
  76.2 1.5 copy.39
  77.7 0.0 reduce-scatter.4.cloned.1.call-update
  77.8 0.0 copy-start.4
  77.8 0.0 copy-start.6
  77.8 66.1 %reduce-scatter.4.cloned.1.call-done = f32[32,1280]{1,0:T(8,128)} async-done(((f32[256,1280]{1,0:T(8,128)}), f32[32,1280]{1,0:T(8,128)}) %reduce-scatter.4.cloned.1.call-update) | async-done | bytes 163856 | tf_op jit(solution)/shard_map/reduce_scatter | solution.py:59
  143.9 1.2 copy.40
  145.1 0.8 multiply_reduce_fusion
  145.9 39.9 %psum.7 = f32[]{:T(128)} all-reduce(f32[]{:T(128)} %multiply_reduce_fusion), channel_id=1, replica_groups=mesh['fs'=8,'tp'=4] {'fs','tp'}, use_global_device_ids=true, to_apply=%region_2.0 | all-reduce | flops 1 | bytes 8 | tf_op jit(solution)/shard_map/psum | solution.py:67
  186.5 0.0 copy-start.10
  186.5 0.0 copy-start.11
  186.5 0.7 divide_convert_fusion
  187.3 31.3 %all_gather.20 = bf16[256,768]{1,0:T(8,128)(2,1)S(1)} all-gather(bf16[32,768]{1,0:T(8,128)(2,1)S(1)} %get-tuple-element.27), channel_id=1, replica_groups=mesh['fs'=8,'tp'=4] {'fs'}, dimensions={0}, use_global_device_ids=true | all-gather | bytes 442368 | tf_op jit(solution)/shard_map/all_gather | solution.py:76
  218.5 0.0 copy-start.7
  218.5 0.9 subtract_convert_fusion
  219.4 32.1 %all_gather.21 = bf16[512,768]{1,0:T(8,128)(2,1)S(1)} all-gather(bf16[64,768]{1,0:T(8,128)(2,1)S(1)} %get-tuple-element.30), channel_id=1, replica_groups=mesh['fs'=8,'tp'=4] {'fs'}, dimensions={0}, use_global_device_ids=true | all-gather | bytes 884736 | tf_op jit(solution)/shard_map/all_gather | solution.py:84
  251.5 0.7 divide_convert_fusion.1
  252.2 30.8 %all_gather.22 = bf16[256,512]{1,0:T(8,128)(2,1)S(1)} all-gather(bf16[32,512]{1,0:T(8,128)(2,1)S(1)} %get-tuple-element.24), channel_id=1, replica_groups=mesh['fs'=8,'tp'=4] {'fs'}, dimensions={0}, use_global_device_ids=true | all-gather | bytes 294912 | tf_op jit(solution)/shard_map/all_gather | solution.py:77
  283.0 0.8 subtract_convert_fusion.1
  283.8 31.2 %all_gather.23 = bf16[512,512]{1,0:T(8,128)(2,1)S(1)} all-gather(bf16[64,512]{1,0:T(8,128)(2,1)S(1)} %get-tuple-element.32), channel_id=1, replica_groups=mesh['fs'=8,'tp'=4] {'fs'}, dimensions={0}, use_global_device_ids=true | all-gather | bytes 589824 | tf_op jit(solution)/shard_map/all_gather | solution.py:85
  315.0 0.9 copy.43
  315.9 0.8 copy.44
  (17 shorter events, 0.1 us)
Async XLA Ops:
  7.2 63.9 %copy-start = (bf16[768,768]{1,0:T(8,128)(2,1)S(1)}, bf16[768,768]{1,0:T(8,128)(2,1)}, u32[]{:S(2)}) copy-start(bf16[768,768]{1,0:T(8,128)(2,1)} %param.13) | copy-start | bytes 3538948
  7.2 136.7 %reduce-scatter.4.cloned.1.call-start = ((), (), s32[]{:S(2)}) async-start(), calls=%async_computation.1 | async-start | bytes 1474560 | tf_op jit(solution)/shard_map/reduce_scatter | solution.py:59
  73.1 1.4 copy-start.1
  73.1 1.4 copy-start.2
  77.7 108.8 %copy-start.8 = (f32[32,768]{1,0:T(8,128)S(1)}, f32[32,768]{1,0:T(8,128)}, u32[]{:S(2)}) copy-start(f32[32,768]{1,0:T(8,128)} %param.17) | copy-start | bytes 294916
  77.7 108.8 %copy-start.9 = (f32[32,768]{1,0:T(8,128)S(1)}, f32[32,768]{1,0:T(8,128)}, u32[]{:S(2)}) copy-start(f32[32,768]{1,0:T(8,128)} %param.16) | copy-start | bytes 294916
  77.8 140.8 %copy-start.4 = (f32[64,768]{1,0:T(8,128)S(1)}, f32[64,768]{1,0:T(8,128)}, u32[]{:S(2)}) copy-start(f32[64,768]{1,0:T(8,128)} %param.14) | copy-start | bytes 589828
  77.8 140.7 %copy-start.6 = (bf16[64,256]{1,0:T(8,128)(2,1)S(1)}, bf16[64,256]{1,0:T(8,128)(2,1)}, u32[]{:S(2)}) copy-start(bf16[64,256]{1,0:T(8,128)(2,1)} %param.15) | copy-start | bytes 98308
  143.9 42.6 %copy-start.3 = (f32[32,1280]{1,0:T(8,128)S(1)}, f32[32,1280]{1,0:T(8,128)}, u32[]{:S(2)}) copy-start(f32[32,1280]{1,0:T(8,128)} %reduce-scatter.4.cloned.1.call-done) | copy-start | bytes 491524
  186.5 65.0 %copy-start.10 = (f32[32,512]{1,0:T(8,128)S(1)}, f32[32,512]{1,0:T(8,128)}, u32[]{:S(2)}) copy-start(f32[32,512]{1,0:T(8,128)} %param.23) | copy-start | bytes 196612
  186.5 65.0 %copy-start.11 = (f32[32,512]{1,0:T(8,128)S(1)}, f32[32,512]{1,0:T(8,128)}, u32[]{:S(2)}) copy-start(f32[32,512]{1,0:T(8,128)} %param.22) | copy-start | bytes 196612
  218.5 64.5 %copy-start.5 = (f32[64,512]{1,0:T(8,128)S(1)}, f32[64,512]{1,0:T(8,128)}, u32[]{:S(2)}) copy-start(f32[64,512]{1,0:T(8,128)} %param.20) | copy-start | bytes 393220
  218.5 64.5 %copy-start.7 = (bf16[64,256]{1,0:T(8,128)(2,1)S(1)}, bf16[64,256]{1,0:T(8,128)(2,1)}, u32[]{:S(2)}) copy-start(bf16[64,256]{1,0:T(8,128)(2,1)} %param.21) | copy-start | bytes 98308
Sparse Core Ops, SparseCore 0:
  77.9 65.9 reduce-scatter.3
where the time goes:
time: 324 us; the launch traced here: 323 us
  blocking collectives  229 us (71%)
  waiting for transfers between devices  66.1 us (20%)
  between operations  14.9 us (5%)
  matrix products  6.67 us (2%)
  local copies, waits for them, and re-layouts  4.45 us (1%)
    reduce_scatter x1, waiting for transfers between devices, body(): lax.psum_scatter(jnp.concatenate([across_latent(q_factor, q_partial), acr...  66.1 us
    psum x1, blocking collectives, body(): squares_sum = lax.psum(jnp.sum(projected * projected), ('fs', 'tp'))  39.9 us
    all_gather x1, blocking collectives, body(): lax.all_gather(uq_basis, 'fs', axis=0, tiled=True)  32.9 us
    all_gather x1, blocking collectives, body(): lax.all_gather(q_fresh, 'fs', axis=0, tiled=True)  32.1 us
    all_gather x1, blocking collectives, body(): lax.all_gather(q_heading, 'fs', axis=0, tiled=True)  31.3 us
    all_gather x1, blocking collectives, body(): lax.all_gather(k_fresh, 'fs', axis=0, tiled=True)  31.2 us
    all_gather x1, blocking collectives, body(): lax.all_gather(uk_basis, 'fs', axis=0, tiled=True)  30.9 us
    all_gather x1, blocking collectives, body(): lax.all_gather(k_heading, 'fs', axis=0, tiled=True)  30.8 us
  transfers between devices with their start and end apart: 1, of which 1 were waited for; matrix products, arithmetic and copies ran while one was open for 0% of the time, Pallas kernels for 0%

commit v1 on v0

--- a/solution.py
+++ b/solution.py
@@ -1,13 +1,424 @@
+import functools
+
 import jax
 import jax.numpy as jnp
 from jax import lax
+from jax.experimental import pallas as pl
+from jax.experimental.pallas import tpu as pltpu
 from jax.sharding import PartitionSpec as P
+
+MESH = pl.DeviceIdType.MESH
+F32 = jnp.float32
+BF16 = jnp.bfloat16
 
 first_decay = 0.8
 second_decay = 0.9
 step_size = 0.5
 mean_guard = 1e-06
 root_guard = 1e-08
+PAIR = 2
+
+
+def transposed_dot(left, right):
+    return lax.dot_general(
+        left, right, (((0,), (0,)), ((), ())), preferred_element_type=F32
+    )
+
+
+def exchange_kernel(
+    n,
+    tp_size,
+    lq_hbm,
+    gq_hbm,
+    lk_hbm,
+    gk_hbm,
+    bq_hbm,
+    bk_hbm,
+    mq_hbm,
+    mk_hbm,
+    fq_hbm,
+    sq_hbm,
+    fk_hbm,
+    sk_hbm,
+    scaled_ref,
+    dir_ref,
+    master_ref,
+    basis_ref,
+    lq,
+    gq,
+    lk,
+    gk,
+    mq,
+    mk,
+    fq,
+    sq,
+    fk,
+    sk,
+    part_q,
+    part_k,
+    proj,
+    px_out,
+    px_in,
+    pz_out,
+    pz_in,
+    st_out,
+    st_in,
+    sf_out,
+    sf_in,
+    local_sem,
+    b_send,
+    b_recv,
+    m_send,
+    m_recv,
+    h_send,
+    h_recv,
+    px_send,
+    px_recv,
+    pz_send,
+    pz_recv,
+    st_send,
+    st_recv,
+    sf_send,
+    sf_recv,
+):
+    outer = n // PAIR
+    me = lax.axis_index("fs")
+    tp = lax.axis_index("tp")
+    z = me // PAIR
+    x = lax.rem(me, PAIR)
+    mate = z * PAIR + (1 - x)
+    width_q = gq.shape[1]
+    latent = n * basis_ref.shape[2]
+    rank = basis_ref.shape[3]
+
+    def level(i):
+        return lax.rem(z + i, outer)
+
+    def remote(src, dst, send, recv, fs_id, tp_id):
+        return pltpu.make_async_remote_copy(
+            src_ref=src,
+            dst_ref=dst,
+            send_sem=send,
+            recv_sem=recv,
+            device_id=(fs_id, tp_id),
+            device_id_type=MESH,
+        )
+
+    loads = []
+    for slot, (src, dst) in enumerate(
+        (
+            (bq_hbm, basis_ref.at[me, 0]),
+            (bk_hbm, basis_ref.at[me, 1]),
+            (mq_hbm, mq),
+            (mk_hbm, mk),
+            (lq_hbm, lq),
+            (gq_hbm, gq),
+            (lk_hbm, lk),
+            (gk_hbm, gk),
+            (fq_hbm, fq),
+            (sq_hbm, sq),
+            (fk_hbm, fk),
+            (sk_hbm, sk),
+        )
+    ):
+        copy = pltpu.make_async_copy(src, dst, local_sem.at[slot])
+        copy.start()
+        loads.append(copy)
+
+    barrier = pltpu.get_barrier_semaphore()
+    for i in range(1, n):
+        pl.semaphore_signal(
+            barrier, inc=1, device_id=(lax.rem(me + i, n), tp), device_id_type=MESH
+        )
+    for i in range(1, tp_size):
+        pl.semaphore_signal(
+            barrier, inc=1, device_id=(me, lax.rem(tp + i, tp_size)), device_id_type=MESH
+        )
+    pl.semaphore_wait(barrier, n - 1 + tp_size - 1)
+
+    pending = []
+
+    def send_own_along(buf, send, recv):
+        for i in range(1, outer):
+            copy = remote(
+                buf.at[me], buf.at[me], send.at[i - 1], recv.at[me], level(i) * PAIR + x, tp
+            )
+            copy.start()
+            pending.append(copy)
+
+    def send_own_across(buf, send, recv):
+        copy = remote(buf.at[me], buf.at[me], send.at[outer - 1], recv.at[me], mate, tp)
+        copy.start()
+        pending.append(copy)
+
+    def forward_across(buf, send, recv, i):
+        source = level(i) * PAIR + x
+        copy = remote(
+            buf.at[source], buf.at[source], send.at[outer - 1 + i], recv.at[source], mate, tp
+        )
+        copy.wait_recv()
+        copy.start()
+        pending.append(copy)
+
+    def wait_across(buf, send, recv):
+        for i in range(outer):
+            source = level(i) * PAIR + (1 - x)
+            remote(
+                buf.at[source], buf.at[source], send.at[0], recv.at[source], mate, tp
+            ).wait_recv()
+
+    loads[0].wait()
+    loads[1].wait()
+    send_own_along(basis_ref, b_send, b_recv)
+    send_own_across(basis_ref, b_send, b_recv)
+
+    loads[2].wait()
+    loads[3].wait()
+    master_ref[me, :, :width_q] = mq[...].astype(BF16)
+    master_ref[me, :, width_q:] = mk[...].astype(BF16)
+    send_own_along(master_ref, m_send, m_recv)
+
+    loads[4].wait()
+    loads[5].wait()
+    part_q[...] = transposed_dot(lq[...], gq[...])
+    loads[6].wait()
+    loads[7].wait()
+    part_k[...] = transposed_dot(lk[...], gk[...])
+
+    for i in range(1, outer):
+        forward_across(basis_ref, b_send, b_recv, i)
+    wait_across(basis_ref, b_send, b_recv)
+
+    def project(which, partial):
+        factor = basis_ref[:, which].reshape(latent, rank)
+        high = partial.astype(BF16)
+        low = (partial - high.astype(F32)).astype(BF16)
+        return transposed_dot(factor, high) + transposed_dot(factor, low)
+
+    rows = rank // n
+    proj[:, :, :width_q] = project(0, part_q[...]).reshape(n, rows, width_q)
+    proj[:, :, width_q:] = project(1, part_k[...]).reshape(n, rows, proj.shape[2] - width_q)
+
+    order = [i for i in range(1, outer)] + [0]
+    for i in order:
+        zd = level(i)
+        px_out[zd] = proj[zd * PAIR + (1 - x)].astype(BF16)
+        copy = remote(px_out.at[zd], px_in.at[zd], px_send.at[zd], px_recv.at[zd], mate, tp)
+        copy.start()
+        pending.append(copy)
+    send_own_across(master_ref, m_send, m_recv)
+
+    def px_wait(zd):
+        remote(
+            px_out.at[zd], px_in.at[zd], px_send.at[zd], px_recv.at[zd], mate, tp
+        ).wait_recv()
+
+    for i in range(1, outer):
+        zd = level(i)
+        px_wait(zd)
+        pz_out[zd] = (proj[zd * PAIR + x] + px_in[zd].astype(F32)).astype(BF16)
+        copy = remote(
+            pz_out.at[zd], pz_in.at[z], pz_send.at[zd], pz_recv.at[z], zd * PAIR + x, tp
+        )
+        copy.start()
+        pending.append(copy)
+    forward_across(master_ref, m_send, m_recv, 1)
+    px_wait(z)
+    total = proj[me] + px_in[z].astype(F32)
+    for i in range(1, outer):
+        zs = level(i)
+        remote(
+            pz_out.at[zs], pz_in.at[zs], pz_send.at[zs], pz_recv.at[zs], zs * PAIR + x, tp
+        ).wait_recv()
+        total = total + pz_in[zs].astype(F32)
+
+    squares = jnp.full(st_out.shape, jnp.sum(total * total), F32)
+    st_out[...] = squares
+    for i in range(1, tp_size):
+        copy = remote(
+            st_out, st_in.at[tp], st_send.at[i], st_recv.at[tp], me, lax.rem(tp + i, tp_size)
+        )
+        copy.start()
+        pending.append(copy)
+    for i in range(1, tp_size):
+        ts = lax.rem(tp + i, tp_size)
+        remote(st_out, st_in.at[ts], st_send.at[i], st_recv.at[ts], me, ts).wait_recv()
+        squares = squares + st_in[ts]
+    sf_out[...] = squares
+    for i in range(1, n):
+        copy = remote(
+            sf_out, sf_in.at[me], sf_send.at[i], sf_recv.at[me], lax.rem(me + i, n), tp
+        )
+        copy.start()
+        pending.append(copy)
+    for i in range(2, outer):
+        forward_across(master_ref, m_send, m_recv, i)
+    for i in range(1, n):
+        fs = lax.rem(me + i, n)
+        remote(sf_out, sf_in.at[fs], sf_send.at[i], sf_recv.at[fs], fs, tp).wait_recv()
+        squares = squares + sf_in[fs]
+
+    count = rows * proj.shape[2] * n * tp_size
+    root_mean = jnp.sqrt(squares / count + mean_guard)[0:1, 0:1]
+    scaled = total / root_mean
+    scaled_ref[...] = scaled
+    for load in loads[8:]:
+        load.wait()
+    dir_ref[me, :, :width_q] = moment_update(scaled[:, :width_q], fq[...], sq[...])[2]
+    dir_ref[me, :, width_q:] = moment_update(scaled[:, width_q:], fk[...], sk[...])[2]
+    send_own_along(dir_ref, h_send, h_recv)
+    send_own_across(dir_ref, h_send, h_recv)
+    for i in range(1, outer):
+        forward_across(dir_ref, h_send, h_recv, i)
+    wait_across(master_ref, m_send, m_recv)
+    wait_across(dir_ref, h_send, h_recv)
+    for copy in pending:
+        copy.wait_send()
+
+
+def apply_kernel(
+    scaled_ref,
+    dir_ref,
+    master_ref,
+    basis_ref,
+    bq,
+    bk,
+    fq,
+    sq,
+    fk,
+    sk,
+    uq_first_new,
+    uq_second_new,
+    uq_step,
+    uq_copy,
+    uk_first_new,
+    uk_second_new,
+    uk_step,
+    uk_copy,
+):
+    n, rows, width = dir_ref.shape
+    deep = basis_ref.shape[2]
+    rank = n * rows
+    width_q = fq.shape[1]
+    for which, cols, own, first, second, first_new, second_new, step, fresh in (
+        (0, slice(0, width_q), bq, fq, sq, uq_first_new, uq_second_new, uq_step, uq_copy),
+        (1, slice(width_q, width), bk, fk, sk, uk_first_new, uk_second_new, uk_step, uk_copy),
+    ):
+        span = cols.stop - cols.start
+        moved = moment_update(scaled_ref[:, cols], first[...], second[...])
+        first_new[...] = moved[0]
+        second_new[...] = moved[1]
+        heading = dir_ref[:, :, cols].reshape(rank, span)
+        step[...] = jnp.dot(own[...], heading, preferred_element_type=F32)
+        factor = basis_ref[:, which].reshape(n * deep, rank)
+        whole = jnp.dot(factor, heading, preferred_element_type=F32)
+        master = master_ref[:, :, cols].reshape(n * deep, span).astype(F32)
+        fresh[...] = (master - step_size * whole).astype(BF16)
+
+
+def kernel_body(
+    n,
+    tp_size,
+    q_latent,
+    q_grad,
+    uq_master,
+    uq_basis,
+    uq_first,
+    uq_second,
+    kv_latent,
+    k_grad,
+    uk_master,
+    uk_basis,
+    uk_first,
+    uk_second,
+):
+    outer = n // PAIR
+    tokens, latent = q_latent.shape
+    deep, rank = uq_basis.shape
+    rows = rank // n
+    width_q, width_k = q_grad.shape[1], k_grad.shape[1]
+    width = width_q + width_k
+    dma = pltpu.SemaphoreType.DMA
+    vmem = pl.BlockSpec(memory_space=pltpu.VMEM)
+    args = (
+        q_latent, q_grad, kv_latent, k_grad, uq_basis, uk_basis,
+        uq_master, uk_master, uq_first, uq_second, uk_first, uk_second,
+    )
+    scaled, heading, master, basis = pl.pallas_call(
+        functools.partial(exchange_kernel, n, tp_size),
+        out_shape=(
+            jax.ShapeDtypeStruct((rows, width), F32),
+            jax.ShapeDtypeStruct((n, rows, width), BF16),
+            jax.ShapeDtypeStruct((n, deep, width), BF16),
+            jax.ShapeDtypeStruct((n, 2, deep, rank), BF16),
+        ),
+        in_specs=[pl.BlockSpec(memory_space=pl.ANY)] * len(args),
+        out_specs=(vmem,) * 4,
+        scratch_shapes=[
+            pltpu.VMEM(q_latent.shape, BF16),
+            pltpu.VMEM(q_grad.shape, BF16),
+            pltpu.VMEM(kv_latent.shape, BF16),
+            pltpu.VMEM(k_grad.shape, BF16),
+            pltpu.VMEM(uq_master.shape, F32),
+            pltpu.VMEM(uk_master.shape, F32),
+            pltpu.VMEM(uq_first.shape, F32),
+            pltpu.VMEM(uq_second.shape, F32),
+            pltpu.VMEM(uk_first.shape, F32),
+            pltpu.VMEM(uk_second.shape, F32),
+            pltpu.VMEM((latent, width_q), F32),
+            pltpu.VMEM((latent, width_k), F32),
+            pltpu.VMEM((n, rows, width), F32),
+            pltpu.VMEM((outer, rows, width), BF16),
+            pltpu.VMEM((outer, rows, width), BF16),
+            pltpu.VMEM((outer, rows, width), BF16),
+            pltpu.VMEM((outer, rows, width), BF16),
+            pltpu.VMEM((8, 128), F32),
+            pltpu.VMEM((tp_size, 8, 128), F32),
+            pltpu.VMEM((8, 128), F32),
+            pltpu.VMEM((n, 8, 128), F32),
+            dma((len(args),)),
+            dma((2 * outer - 1,)),
+            dma((n,)),
+            dma((2 * outer - 1,)),
+            dma((n,)),
+            dma((2 * outer - 1,)),
+            dma((n,)),
+            dma((outer,)),
+            dma((outer,)),
+            dma((outer,)),
+            dma((outer,)),
+            dma((tp_size,)),
+            dma((tp_size,)),
+            dma((n,)),
+            dma((n,)),
+        ],
+        compiler_params=pltpu.CompilerParams(
+            collective_id=0, has_side_effects=True, vmem_limit_bytes=40 * 1024 * 1024
+        ),
+        name="exchange",
+    )(*args)
+    shapes = tuple(
+        jax.ShapeDtypeStruct(shape, dtype)
+        for span in (width_q, width_k)
+        for shape, dtype in (
+            ((rows, span), F32),
+            ((rows, span), F32),
+            ((deep, span), F32),
+            ((latent, span), BF16),
+        )
+    )
+    return tuple(
+        pl.pallas_call(
+            apply_kernel,
+            out_shape=shapes,
+            in_specs=[vmem] * 10,
+            out_specs=(vmem,) * 8,
+            name="apply",
+        )(
+            scaled, heading, master, basis, uq_basis, uk_basis,
+            uq_first, uq_second, uk_first, uk_second,
+        )
+    )
 
 
 def across_tokens(left, right):
@@ -96,9 +507,18 @@
     )
 
 
+def chosen_body(n, tp_size, *args):
+    deep, rank = args[3].shape
+    tiled = n % PAIR == 0 and rank % (16 * n) == 0 and deep % 16 == 0
+    lanes = args[1].shape[1] % 128 == 0 and args[7].shape[1] % 128 == 0 and rank % 128 == 0
+    if tiled and lanes:
+        return kernel_body(n, tp_size, *args)
+    return body(*args)
+
+
 def solution(mesh):
     return jax.shard_map(
-        body,
+        functools.partial(chosen_body, mesh.shape["fs"], mesh.shape["tp"]),
         mesh=mesh,
         in_specs=(
             P("fs", None),

time: 324 us -> 79.5 us (0.25)
  blocking collectives: 229 us -> 0 us
  waiting for transfers between devices: 66.1 us -> 0 us
  Pallas kernels: 0 us -> 63.3 us
  between operations: 14.9 us -> 0.67 us
  local copies, waits for them, and re-layouts: 4.45 us -> 14.8 us
  matrix products: 6.67 us -> 0 us
    all_gather x6 -> x0, blocking collectives: 189 us -> none  [the longest x1 32.9 us: body(): lax.all_gather(uq_basis, 'fs', axis=0, tiled=True)]
    reduce_scatter x1 -> x0, waiting for transfers between devices: 66.1 us -> none  [body(): lax.psum_scatter(jnp.concatenate([across_latent(q_factor, q_partial), acr...]
    pallas_call x0 -> x2, Pallas kernels: none -> 63.3 us  [the longest x1 59.8 us: kernel_body(): pl.pallas_call(functools.partial(exchange_kernel, n, tp_size), out_shape=...]
    psum x1 -> x0, blocking collectives: 39.9 us -> none  [body(): squares_sum = lax.psum(jnp.sum(projected * projected), ('fs', 'tp'))]
    unnamed x28 -> x32, local copies, waits for them, and re-layouts: 4.45 us -> 14.8 us
    dot_general x6 -> x0, matrix products: 6.67 us -> none  [the longest x2 2.55 us: across_tokens(): lax.dot_general(left, right, (((0,), (0,)), ((), ())), preferred_element_...]
  transfers between devices with their start and end apart: 1 -> 0, of which waited for: 1 -> 0; matrix products, arithmetic and copies ran while one was open for 0% -> 0% of each run, Pallas kernels for 0% -> 0%
where the time goes in v1:
time: 79.5 us; the launch traced here: 78.8 us
  Pallas kernels  63.3 us (80%)
  local copies, waits for them, and re-layouts  14.8 us (19%)
    pallas_call x1, Pallas kernels, kernel_body(): pl.pallas_call(functools.partial(exchange_kernel, n, tp_size), out_shape=...  59.8 us
    unnamed x32, local copies, waits for them, and re-layouts  14.8 us
    pallas_call x1, Pallas kernels, kernel_body(): pl.pallas_call(apply_kernel, out_shape=shapes, in_specs=[vmem] * 10, out_...  3.53 us

profile of v1, /device:TPU:0, one launch (start us, length us, event | category | flops | bytes accessed | tf_op | source)
XLA Modules:
  0.0 78.8 jit_solution(7933833647305546502)
XLA Ops:
  0.6 0.0 copy-start.1
  0.6 1.3 %copy-done.1 = bf16[768,768]{1,0:T(8,128)(2,1)S(1)} copy-done((bf16[768,768]{1,0:T(8,128)(2,1)S(1)}, bf16[768,768]{1,0:T(8,128)(2,1)}, u32[]{:S(2)}) %copy-start.1) | copy-done | bytes 1179672
  1.9 0.0 copy-start.2
  1.9 1.1 %copy-done.2 = bf16[768,512]{1,0:T(8,128)(2,1)S(1)} copy-done((bf16[768,512]{1,0:T(8,128)(2,1)S(1)}, bf16[768,512]{1,0:T(8,128)(2,1)}, u32[]{:S(2)}) %copy-start.2) | copy-done | bytes 786456
  3.0 1.1 %copy-done.3 = bf16[768,512]{1,0:T(8,128)(2,1)S(1)} copy-done((bf16[768,512]{1,0:T(8,128)(2,1)S(1)}, bf16[768,512]{1,0:T(8,128)(2,1)}, u32[]{:S(2)}) %copy-start.3) | copy-done | bytes 786456
  4.2 0.0 copy-start.4
  4.2 1.1 %copy-done.4 = bf16[768,512]{1,0:T(8,128)(2,1)S(1)} copy-done((bf16[768,512]{1,0:T(8,128)(2,1)S(1)}, bf16[768,512]{1,0:T(8,128)(2,1)}, u32[]{:S(2)}) %copy-start.4) | copy-done | bytes 786456
  5.3 0.0 copy-start.7
  5.3 0.9 %copy-done.7 = f32[32,768]{1,0:T(8,128)S(1)} copy-done((f32[32,768]{1,0:T(8,128)S(1)}, f32[32,768]{1,0:T(8,128)}, u32[]{:S(2)}) %copy-start.7) | copy-done | bytes 98328
  6.2 0.0 copy-start.8
  6.2 0.9 %copy-done.8 = f32[32,768]{1,0:T(8,128)S(1)} copy-done((f32[32,768]{1,0:T(8,128)S(1)}, f32[32,768]{1,0:T(8,128)}, u32[]{:S(2)}) %copy-start.8) | copy-done | bytes 98328
  7.1 0.0 copy-start.9
  7.1 0.8 %copy-done.9 = f32[32,512]{1,0:T(8,128)S(1)} copy-done((f32[32,512]{1,0:T(8,128)S(1)}, f32[32,512]{1,0:T(8,128)}, u32[]{:S(2)}) %copy-start.9) | copy-done | bytes 65560
  7.9 0.0 copy-start.10
  7.9 0.8 %copy-done.10 = f32[32,512]{1,0:T(8,128)S(1)} copy-done((f32[32,512]{1,0:T(8,128)S(1)}, f32[32,512]{1,0:T(8,128)}, u32[]{:S(2)}) %copy-start.10) | copy-done | bytes 65560
  8.8 0.0 copy-start.11
  8.8 0.9 %copy-done.11 = f32[64,768]{1,0:T(8,128)S(1)} copy-done((f32[64,768]{1,0:T(8,128)S(1)}, f32[64,768]{1,0:T(8,128)}, u32[]{:S(2)}) %copy-start.11) | copy-done | bytes 196632
  9.7 0.0 copy-start.13
  9.7 0.8 copy-done.13
  10.5 0.0 copy-start.14
  10.5 0.8 copy-done.14
  11.2 0.0 copy-start.15
  11.2 0.9 %copy-done.15 = f32[64,512]{1,0:T(8,128)S(1)} copy-done((f32[64,512]{1,0:T(8,128)S(1)}, f32[64,512]{1,0:T(8,128)}, u32[]{:S(2)}) %copy-start.15) | copy-done | bytes 131096
  12.1 59.8 %exchange.1 = (f32[32,1280]{1,0:T(8,128)S(1)}, bf16[8,32,1280]{2,1,0:T(8,128)(2,1)S(1)}, bf16[8,64,1280]{2,1,0:T(8,128)(2,1)S(1)}, bf16[8,2,64,256]{3,2,1,0:T(8,128)(2,1)S(1)}) custom-call(bf16[768,512]{1,0:T(8,128)(2,1)S(1)} %copy-done.2, bf16[768,768]{1,0:T(8,128)(2,1)S(1)} %copy-done.1, bf16[768,512]{1,0:T(8,128)(2,1)S(1)} %copy-done.3, ...), custom_call_target="tpu_custom_call" | custom-call | tf_op jit(solution)/shard_map/exchange/pallas_call | solution.py:347
  71.9 0.0 copy-start
  71.9 1.1 %copy-done = bf16[8,64,1280]{2,1,0:T(8,128)(2,1)} copy-done((bf16[8,64,1280]{2,1,0:T(8,128)(2,1)}, bf16[8,64,1280]{2,1,0:T(8,128)(2,1)S(1)}, u32[]{:S(2)}) %copy-start) | copy-done | bytes 1310744
  73.0 0.0 copy-start.5
  73.0 0.8 %copy-done.5 = bf16[8,32,1280]{2,1,0:T(8,128)(2,1)} copy-done((bf16[8,32,1280]{2,1,0:T(8,128)(2,1)}, bf16[8,32,1280]{2,1,0:T(8,128)(2,1)S(1)}, u32[]{:S(2)}) %copy-start.5) | copy-done | bytes 655384
  73.8 0.0 copy-start.6
  73.8 0.8 %copy-done.6 = bf16[8,2,64,256]{3,2,1,0:T(8,128)(2,1)} copy-done((bf16[8,2,64,256]{3,2,1,0:T(8,128)(2,1)}, bf16[8,2,64,256]{3,2,1,0:T(8,128)(2,1)S(1)}, u32[]{:S(2)}) %copy-start.6) | copy-done | bytes 524312
  74.6 0.7 copy-done.12
  75.3 3.5 %apply.1 = (f32[32,768]{1,0:T(8,128)}, f32[32,768]{1,0:T(8,128)}, f32[64,768]{1,0:T(8,128)}, bf16[512,768]{1,0:T(8,128)(2,1)}, f32[32,512]{1,0:T(8,128)}, /*inde...) custom-call(f32[32,1280]{1,0:T(8,128)} %copy-done.12, bf16[8,32,1280]{2,1,0:T(8,128)(2,1)} %copy-done.5, ...), custom_call_target="tpu_custom_call" | custom-call | tf_op jit(solution)/shard_map/apply/pallas_call | solution.py:411
  (2 shorter events, 0.0 us)
Async XLA Ops:
  0.6 1.3 %copy-start.1 = (bf16[768,768]{1,0:T(8,128)(2,1)S(1)}, bf16[768,768]{1,0:T(8,128)(2,1)}, u32[]{:S(2)}) copy-start(bf16[768,768]{1,0:T(8,128)(2,1)} %gq_hbm.1) | copy-start | bytes 3538948
  1.9 1.1 %copy-start.2 = (bf16[768,512]{1,0:T(8,128)(2,1)S(1)}, bf16[768,512]{1,0:T(8,128)(2,1)}, u32[]{:S(2)}) copy-start(bf16[768,512]{1,0:T(8,128)(2,1)} %lq_hbm.1) | copy-start | bytes 2359300
  3.0 1.1 %copy-start.3 = (bf16[768,512]{1,0:T(8,128)(2,1)S(1)}, bf16[768,512]{1,0:T(8,128)(2,1)}, u32[]{:S(2)}) copy-start(bf16[768,512]{1,0:T(8,128)(2,1)} %lk_hbm.1) | copy-start | bytes 2359300
  4.2 1.1 %copy-start.4 = (bf16[768,512]{1,0:T(8,128)(2,1)S(1)}, bf16[768,512]{1,0:T(8,128)(2,1)}, u32[]{:S(2)}) copy-start(bf16[768,512]{1,0:T(8,128)(2,1)} %gk_hbm.1) | copy-start | bytes 2359300
  5.3 0.9 %copy-start.7 = (f32[32,768]{1,0:T(8,128)S(1)}, f32[32,768]{1,0:T(8,128)}, u32[]{:S(2)}) copy-start(f32[32,768]{1,0:T(8,128)} %fq.1) | copy-start | bytes 294916
  6.2 0.9 %copy-start.8 = (f32[32,768]{1,0:T(8,128)S(1)}, f32[32,768]{1,0:T(8,128)}, u32[]{:S(2)}) copy-start(f32[32,768]{1,0:T(8,128)} %sq.1) | copy-start | bytes 294916
  7.1 0.8 %copy-start.9 = (f32[32,512]{1,0:T(8,128)S(1)}, f32[32,512]{1,0:T(8,128)}, u32[]{:S(2)}) copy-start(f32[32,512]{1,0:T(8,128)} %fk.1) | copy-start | bytes 196612
  7.9 0.8 %copy-start.10 = (f32[32,512]{1,0:T(8,128)S(1)}, f32[32,512]{1,0:T(8,128)}, u32[]{:S(2)}) copy-start(f32[32,512]{1,0:T(8,128)} %sk.1) | copy-start | bytes 196612
  8.8 0.9 %copy-start.11 = (f32[64,768]{1,0:T(8,128)S(1)}, f32[64,768]{1,0:T(8,128)}, u32[]{:S(2)}) copy-start(f32[64,768]{1,0:T(8,128)} %mq_hbm.1) | copy-start | bytes 589828
  9.7 0.8 copy-start.13
  10.5 0.8 copy-start.14
  11.2 0.9 %copy-start.15 = (f32[64,512]{1,0:T(8,128)S(1)}, f32[64,512]{1,0:T(8,128)}, u32[]{:S(2)}) copy-start(f32[64,512]{1,0:T(8,128)} %mk_hbm.1) | copy-start | bytes 393220
  71.9 1.1 %copy-start = (bf16[8,64,1280]{2,1,0:T(8,128)(2,1)}, bf16[8,64,1280]{2,1,0:T(8,128)(2,1)S(1)}, u32[]{:S(2)}) copy-start(bf16[8,64,1280]{2,1,0:T(8,128)(2,1)S(1)} %get-tuple-element.14.master_ref) | copy-start | bytes 3932164
  73.0 0.8 %copy-start.5 = (bf16[8,32,1280]{2,1,0:T(8,128)(2,1)}, bf16[8,32,1280]{2,1,0:T(8,128)(2,1)S(1)}, u32[]{:S(2)}) copy-start(bf16[8,32,1280]{2,1,0:T(8,128)(2,1)S(1)} %get-tuple-element.13.dir_ref) | copy-start | bytes 1966084
  73.8 0.8 %copy-start.6 = (bf16[8,2,64,256]{3,2,1,0:T(8,128)(2,1)}, bf16[8,2,64,256]{3,2,1,0:T(8,128)(2,1)S(1)}, u32[]{:S(2)}) copy-start(bf16[8,2,64,256]{3,2,1,0:T(8,128)(2,1)S(1)} %get-tuple-element.15.basis_ref) | copy-start | bytes 1572868
  74.6 0.7 copy-start.12

commit v2 on v1

--- a/solution.py
+++ b/solution.py
@@ -17,6 +17,7 @@
 mean_guard = 1e-06
 root_guard = 1e-08
 PAIR = 2
+VMEM_BYTES = 67043328
 
 
 def transposed_dot(left, right):
@@ -40,6 +41,10 @@
     sq_hbm,
     fk_hbm,
     sk_hbm,
+    scaled_out,
+    dir_out,
+    master_out,
+    basis_out,
     scaled_ref,
     dir_ref,
     master_ref,
@@ -66,8 +71,12 @@
     sf_out,
     sf_in,
     local_sem,
+    out_sem,
+    dir_sem,
     b_send,
     b_recv,
+    c_send,
+    c_recv,
     m_send,
     m_recv,
     h_send,
@@ -87,6 +96,8 @@
     z = me // PAIR
     x = lax.rem(me, PAIR)
     mate = z * PAIR + (1 - x)
+    which = lax.rem(tp, PAIR)
+    twin = tp + 1 - 2 * which
     width_q = gq.shape[1]
     latent = n * basis_ref.shape[2]
     rank = basis_ref.shape[3]
@@ -138,45 +149,70 @@
 
     pending = []
 
-    def send_own_along(buf, send, recv):
-        for i in range(1, outer):
-            copy = remote(
-                buf.at[me], buf.at[me], send.at[i - 1], recv.at[me], level(i) * PAIR + x, tp
-            )
+    def start(copy, when=None):
+        if when is None:
             copy.start()
-            pending.append(copy)
-
-    def send_own_across(buf, send, recv):
-        copy = remote(buf.at[me], buf.at[me], send.at[outer - 1], recv.at[me], mate, tp)
+        else:
+            pl.when(when)(copy.start)
+        pending.append((copy, when))
+
+    def send_out(src, dst, sem):
+        copy = pltpu.make_async_copy(src, dst, sem)
         copy.start()
-        pending.append(copy)
-
-    def forward_across(buf, send, recv, i):
-        source = level(i) * PAIR + x
-        copy = remote(
-            buf.at[source], buf.at[source], send.at[outer - 1 + i], recv.at[source], mate, tp
-        )
-        copy.wait_recv()
-        copy.start()
-        pending.append(copy)
-
-    def wait_across(buf, send, recv):
-        for i in range(outer):
-            source = level(i) * PAIR + (1 - x)
-            remote(
-                buf.at[source], buf.at[source], send.at[0], recv.at[source], mate, tp
-            ).wait_recv()
+        stores.append(copy)
+
+    stores = []
+
+    def basis_copy(source, send, fs_id):
+        slot = basis_ref.at[source, which]
+        return remote(slot, slot, b_send.at[send], b_recv.at[source], fs_id, tp)
+
+    def to_twin(source):
+        slot = basis_ref.at[source, which]
+        start(remote(slot, slot, c_send.at[source], c_recv.at[source], me, twin))
 
     loads[0].wait()
     loads[1].wait()
-    send_own_along(basis_ref, b_send, b_recv)
-    send_own_across(basis_ref, b_send, b_recv)
+    for i in range(1, outer):
+        start(basis_copy(me, i - 1, level(i) * PAIR + x))
+    start(basis_copy(me, outer - 1, mate))
 
     loads[2].wait()
     loads[3].wait()
     master_ref[me, :, :width_q] = mq[...].astype(BF16)
     master_ref[me, :, width_q:] = mk[...].astype(BF16)
-    send_own_along(master_ref, m_send, m_recv)
+
+    def master_copy(source, send, fs_id):
+        slot = master_ref.at[source]
+        return remote(slot, slot, m_send.at[send], m_recv.at[source], fs_id, tp)
+
+    def toward(sign, hop):
+        holds = (z >= hop) if sign > 0 else (z + hop < outer)
+        room = (z + 1 < outer) if sign > 0 else (z >= 1)
+        near = level(outer + sign) * PAIR + x
+        source = level(outer - sign * hop) * PAIR + x
+        return holds, room, near, source
+
+    def send_master_along(hop):
+        for side, sign in enumerate((1, -1)):
+            holds, room, near, source = toward(sign, hop)
+            if hop:
+                copy = master_copy(source, 0, near)
+                pl.when(holds)(copy.wait_recv)
+            if hop < outer - 1:
+                copy = master_copy(source, 2 * hop + side, near)
+                start(copy, jnp.logical_and(holds, room) if hop else room)
+
+    def send_master_across(hop):
+        base = 2 * (outer - 1)
+        if hop == 0:
+            start(master_copy(me, base, mate))
+            return
+        for side, sign in enumerate((1, -1)):
+            holds, _, _, source = toward(sign, hop)
+            start(master_copy(source, base + 2 * hop - 1 + side, mate), holds)
+
+    send_master_along(0)
 
     loads[4].wait()
     loads[5].wait()
@@ -186,11 +222,24 @@
     part_k[...] = transposed_dot(lk[...], gk[...])
 
     for i in range(1, outer):
-        forward_across(basis_ref, b_send, b_recv, i)
-    wait_across(basis_ref, b_send, b_recv)
-
-    def project(which, partial):
-        factor = basis_ref[:, which].reshape(latent, rank)
+        source = level(i) * PAIR + x
+        copy = basis_copy(source, outer - 1 + i, mate)
+        copy.wait_recv()
+        start(copy)
+        to_twin(source)
+    send_master_across(0)
+    for i in range(outer):
+        source = level(i) * PAIR + (1 - x)
+        basis_copy(source, 0, mate).wait_recv()
+        to_twin(source)
+    for i in range(1, n):
+        source = lax.rem(me + i, n)
+        slot = basis_ref.at[source, 1 - which]
+        remote(slot, slot, c_send.at[source], c_recv.at[source], me, twin).wait_recv()
+    send_out(basis_ref, basis_out, out_sem.at[0])
+
+    def project(side, partial):
+        factor = basis_ref[:, side].reshape(latent, rank)
         high = partial.astype(BF16)
         low = (partial - high.astype(F32)).astype(BF16)
         return transposed_dot(factor, high) + transposed_dot(factor, low)
@@ -203,10 +252,10 @@
     for i in order:
         zd = level(i)
         px_out[zd] = proj[zd * PAIR + (1 - x)].astype(BF16)
-        copy = remote(px_out.at[zd], px_in.at[zd], px_send.at[zd], px_recv.at[zd], mate, tp)
-        copy.start()
-        pending.append(copy)
-    send_own_across(master_ref, m_send, m_recv)
+        start(remote(px_out.at[zd], px_in.at[zd], px_send.at[zd], px_recv.at[zd], mate, tp))
+        if i == 1:
+            send_master_along(1)
+    send_master_across(1)
 
     def px_wait(zd):
         remote(
@@ -217,12 +266,14 @@
         zd = level(i)
         px_wait(zd)
         pz_out[zd] = (proj[zd * PAIR + x] + px_in[zd].astype(F32)).astype(BF16)
-        copy = remote(
-            pz_out.at[zd], pz_in.at[z], pz_send.at[zd], pz_recv.at[z], zd * PAIR + x, tp
-        )
-        copy.start()
-        pending.append(copy)
-    forward_across(master_ref, m_send, m_recv, 1)
+        start(
+            remote(pz_out.at[zd], pz_in.at[z], pz_send.at[zd], pz_recv.at[z], zd * PAIR + x, tp)
+        )
+        if i == 1:
+            for hop in range(2, outer - 1):
+                send_master_along(hop)
+    for hop in range(2, outer - 1):
+        send_master_across(hop)
     px_wait(z)
     total = proj[me] + px_in[z].astype(F32)
     for i in range(1, outer):
@@ -235,24 +286,22 @@
     squares = jnp.full(st_out.shape, jnp.sum(total * total), F32)
     st_out[...] = squares
     for i in range(1, tp_size):
-        copy = remote(
-            st_out, st_in.at[tp], st_send.at[i], st_recv.at[tp], me, lax.rem(tp + i, tp_size)
-        )
-        copy.start()
-        pending.append(copy)
+        start(
+            remote(
+                st_out, st_in.at[tp], st_send.at[i], st_recv.at[tp], me, lax.rem(tp + i, tp_size)
+            )
+        )
     for i in range(1, tp_size):
         ts = lax.rem(tp + i, tp_size)
         remote(st_out, st_in.at[ts], st_send.at[i], st_recv.at[ts], me, ts).wait_recv()
         squares = squares + st_in[ts]
     sf_out[...] = squares
     for i in range(1, n):
-        copy = remote(
-            sf_out, sf_in.at[me], sf_send.at[i], sf_recv.at[me], lax.rem(me + i, n), tp
-        )
-        copy.start()
-        pending.append(copy)
-    for i in range(2, outer):
-        forward_across(master_ref, m_send, m_recv, i)
+        start(
+            remote(sf_out, sf_in.at[me], sf_send.at[i], sf_recv.at[me], lax.rem(me + i, n), tp)
+        )
+    send_master_along(outer - 1)
+    send_master_across(outer - 1)
     for i in range(1, n):
         fs = lax.rem(me + i, n)
         remote(sf_out, sf_in.at[fs], sf_send.at[i], sf_recv.at[fs], fs, tp).wait_recv()
@@ -266,14 +315,39 @@
         load.wait()
     dir_ref[me, :, :width_q] = moment_update(scaled[:, :width_q], fq[...], sq[...])[2]
     dir_ref[me, :, width_q:] = moment_update(scaled[:, width_q:], fk[...], sk[...])[2]
-    send_own_along(dir_ref, h_send, h_recv)
-    send_own_across(dir_ref, h_send, h_recv)
+    def dir_copy(source, send, fs_id):
+        slot = dir_ref.at[source]
+        return remote(slot, slot, h_send.at[send], h_recv.at[source], fs_id, tp)
+
+    def dir_store(source):
+        send_out(dir_ref.at[source], dir_out.at[source], dir_sem.at[source])
+
     for i in range(1, outer):
-        forward_across(dir_ref, h_send, h_recv, i)
-    wait_across(master_ref, m_send, m_recv)
-    wait_across(dir_ref, h_send, h_recv)
-    for copy in pending:
-        copy.wait_send()
+        start(dir_copy(me, i - 1, level(i) * PAIR + x))
+    start(dir_copy(me, outer - 1, mate))
+    send_out(scaled_ref, scaled_out, out_sem.at[1])
+    dir_store(me)
+    for i in range(outer):
+        source = level(i) * PAIR + (1 - x)
+        master_copy(source, 0, mate).wait_recv()
+    send_out(master_ref, master_out, out_sem.at[2])
+    for i in range(1, outer):
+        source = level(i) * PAIR + x
+        copy = dir_copy(source, outer - 1 + i, mate)
+        copy.wait_recv()
+        start(copy)
+        dir_store(source)
+    for i in range(outer):
+        source = level(i) * PAIR + (1 - x)
+        dir_copy(source, 0, mate).wait_recv()
+        dir_store(source)
+    for copy, when in pending:
+        if when is None:
+            copy.wait_send()
+        else:
+            pl.when(when)(copy.wait_send)
+    for copy in stores:
+        copy.wait()
 
 
 def apply_kernel(
@@ -353,8 +427,12 @@
             jax.ShapeDtypeStruct((n, 2, deep, rank), BF16),
         ),
         in_specs=[pl.BlockSpec(memory_space=pl.ANY)] * len(args),
-        out_specs=(vmem,) * 4,
+        out_specs=(pl.BlockSpec(memory_space=pl.ANY),) * 4,
         scratch_shapes=[
+            pltpu.VMEM((rows, width), F32),
+            pltpu.VMEM((n, rows, width), BF16),
+            pltpu.VMEM((n, deep, width), BF16),
+            pltpu.VMEM((n, 2, deep, rank), BF16),
             pltpu.VMEM(q_latent.shape, BF16),
             pltpu.VMEM(q_grad.shape, BF16),
             pltpu.VMEM(kv_latent.shape, BF16),
@@ -377,9 +455,13 @@
             pltpu.VMEM((8, 128), F32),
             pltpu.VMEM((n, 8, 128), F32),
             dma((len(args),)),
+            dma((3,)),
+            dma((n,)),
             dma((2 * outer - 1,)),
             dma((n,)),
-            dma((2 * outer - 1,)),
+            dma((n,)),
+            dma((n,)),
+            dma((4 * outer - 3,)),
             dma((n,)),
             dma((2 * outer - 1,)),
             dma((n,)),
@@ -393,7 +475,7 @@
             dma((n,)),
         ],
         compiler_params=pltpu.CompilerParams(
-            collective_id=0, has_side_effects=True, vmem_limit_bytes=40 * 1024 * 1024
+            collective_id=0, has_side_effects=True, vmem_limit_bytes=VMEM_BYTES
         ),
         name="exchange",
     )(*args)
@@ -509,7 +591,7 @@
 
 def chosen_body(n, tp_size, *args):
     deep, rank = args[3].shape
-    tiled = n % PAIR == 0 and rank % (16 * n) == 0 and deep % 16 == 0
+    tiled = n > 2 * PAIR and n % PAIR == 0 and tp_size % PAIR == 0 and rank % (16 * n) == 0 and deep % 16 == 0
     lanes = args[1].shape[1] % 128 == 0 and args[7].shape[1] % 128 == 0 and rank % 128 == 0
     if tiled and lanes:
         return kernel_body(n, tp_size, *args)

time: 79.5 us -> 56.6 us (0.71)
  local copies, waits for them, and re-layouts: 14.8 us -> 0 us
  Pallas kernels: 63.3 us -> 55.8 us
    unnamed x32 -> x0, local copies, waits for them, and re-layouts: 14.8 us -> none
    pallas_call x1, Pallas kernels: 59.8 us -> 52.3 us  [kernel_body(): pl.pallas_call(functools.partial(exchange_kernel, n, tp_size), out_shape=...]
where the time goes in v2:
time: 56.6 us; the launch traced here: 56.5 us
  Pallas kernels  55.8 us (99%)
  between operations  0.64 us (1%)
    pallas_call x1, Pallas kernels, kernel_body(): pl.pallas_call(functools.partial(exchange_kernel, n, tp_size), out_shape=...  52.3 us
    pallas_call x1, Pallas kernels, kernel_body(): pl.pallas_call(apply_kernel, out_shape=shapes, in_specs=[vmem] * 10, out_...  3.53 us

profile of v2, /device:TPU:0, one launch (start us, length us, event | category | flops | bytes accessed | tf_op | source)
XLA Modules:
  0.0 56.5 jit_solution(15203459867707658972)
XLA Ops:
  0.6 52.3 %exchange.1 = (f32[32,1280]{1,0:T(8,128)}, bf16[8,32,1280]{2,1,0:T(8,128)(2,1)}, bf16[8,64,1280]{2,1,0:T(8,128)(2,1)}, bf16[8,2,64,256]{3,2,1,0:T(8,128)(2,1)}) custom-call(bf16[768,512]{1,0:T(8,128)(2,1)} %lq_hbm.1, bf16[768,768]{1,0:T(8,128)(2,1)} %gq_hbm.1, bf16[768,512]{1,0:T(8,128)(2,1)} %lk_hbm.1, bf16[768,512]{1,0:T(8,128)(2,1)} %gk_hbm.1, ...), custom_call_target="tpu_custom_call" | custom-call | tf_op jit(solution)/shard_map/exchange/pallas_call | solution.py:421
  52.9 3.5 %apply.1 = (f32[32,768]{1,0:T(8,128)}, f32[32,768]{1,0:T(8,128)}, f32[64,768]{1,0:T(8,128)}, bf16[512,768]{1,0:T(8,128)(2,1)}, f32[32,512]{1,0:T(8,128)}, /*inde...) custom-call(f32[32,1280]{1,0:T(8,128)} %get-tuple-element.12.scaled_ref, ...), custom_call_target="tpu_custom_call" | custom-call | tf_op jit(solution)/shard_map/apply/pallas_call | solution.py:493

commit v3 on v2

--- a/solution.py
+++ b/solution.py
@@ -245,42 +245,59 @@
         return transposed_dot(factor, high) + transposed_dot(factor, low)
 
     rows = rank // n
-    proj[:, :, :width_q] = project(0, part_q[...]).reshape(n, rows, width_q)
-    proj[:, :, width_q:] = project(1, part_k[...]).reshape(n, rows, proj.shape[2] - width_q)
+    width = proj.shape[2]
+    pieces = (slice(0, width_q), slice(width_q, width))
+    partials = (part_q, part_k)
+
+    def px_copy(zd, side):
+        cols = pieces[side]
+        return remote(
+            px_out.at[zd, :, cols],
+            px_in.at[zd, :, cols],
+            px_send.at[zd, side],
+            px_recv.at[zd, side],
+            mate,
+            tp,
+        )
+
+    def pz_copy(zd, zs, side):
+        cols = pieces[side]
+        return remote(
+            pz_out.at[zd, :, cols],
+            pz_in.at[zs, :, cols],
+            pz_send.at[zd, side],
+            pz_recv.at[zs, side],
+            zd * PAIR + x,
+            tp,
+        )
 
     order = [i for i in range(1, outer)] + [0]
-    for i in order:
-        zd = level(i)
-        px_out[zd] = proj[zd * PAIR + (1 - x)].astype(BF16)
-        start(remote(px_out.at[zd], px_in.at[zd], px_send.at[zd], px_recv.at[zd], mate, tp))
-        if i == 1:
-            send_master_along(1)
+    for side, cols in enumerate(pieces):
+        span = cols.stop - cols.start
+        proj[:, :, cols] = project(side, partials[side][...]).reshape(n, rows, span)
+        for i in order:
+            zd = level(i)
+            px_out[zd, :, cols] = proj[zd * PAIR + (1 - x), :, cols].astype(BF16)
+            start(px_copy(zd, side))
+    send_master_along(1)
     send_master_across(1)
 
-    def px_wait(zd):
-        remote(
-            px_out.at[zd], px_in.at[zd], px_send.at[zd], px_recv.at[zd], mate, tp
-        ).wait_recv()
-
-    for i in range(1, outer):
-        zd = level(i)
-        px_wait(zd)
-        pz_out[zd] = (proj[zd * PAIR + x] + px_in[zd].astype(F32)).astype(BF16)
-        start(
-            remote(pz_out.at[zd], pz_in.at[z], pz_send.at[zd], pz_recv.at[z], zd * PAIR + x, tp)
-        )
-        if i == 1:
-            for hop in range(2, outer - 1):
-                send_master_along(hop)
+    for side, cols in enumerate(pieces):
+        for i in range(1, outer):
+            zd = level(i)
+            px_copy(zd, side).wait_recv()
+            pz_out[zd, :, cols] = (
+                proj[zd * PAIR + x, :, cols] + px_in[zd, :, cols].astype(F32)
+            ).astype(BF16)
+            start(pz_copy(zd, z, side))
+        px_copy(z, side).wait_recv()
     for hop in range(2, outer - 1):
-        send_master_across(hop)
-    px_wait(z)
+        send_master_along(hop)
     total = proj[me] + px_in[z].astype(F32)
     for i in range(1, outer):
         zs = level(i)
-        remote(
-            pz_out.at[zs], pz_in.at[zs], pz_send.at[zs], pz_recv.at[zs], zs * PAIR + x, tp
-        ).wait_recv()
+        for side in range(len(pieces)):
+            pz_copy(zs, zs, side).wait_recv()
         total = total + pz_in[zs].astype(F32)
 
     squares = jnp.full(st_out.shape, jnp.sum(total * total), F32)
@@ -300,6 +317,8 @@
         start(
             remote(sf_out, sf_in.at[me], sf_send.at[i], sf_recv.at[me], lax.rem(me + i, n), tp)
         )
+    for hop in range(2, outer - 1):
+        send_master_across(hop)
     send_master_along(outer - 1)
     send_master_across(outer - 1)
     for i in range(1, n):
@@ -307,39 +326,44 @@
         remote(sf_out, sf_in.at[fs], sf_send.at[i], sf_recv.at[fs], fs, tp).wait_recv()
         squares = squares + sf_in[fs]
 
-    count = rows * proj.shape[2] * n * tp_size
+    count = rows * width * n * tp_size
     root_mean = jnp.sqrt(squares / count + mean_guard)[0:1, 0:1]
     scaled = total / root_mean
     scaled_ref[...] = scaled
     for load in loads[8:]:
         load.wait()
-    dir_ref[me, :, :width_q] = moment_update(scaled[:, :width_q], fq[...], sq[...])[2]
-    dir_ref[me, :, width_q:] = moment_update(scaled[:, width_q:], fk[...], sk[...])[2]
-    def dir_copy(source, send, fs_id):
-        slot = dir_ref.at[source]
-        return remote(slot, slot, h_send.at[send], h_recv.at[source], fs_id, tp)
+    def dir_copy(source, send, fs_id, side):
+        slot = dir_ref.at[source, :, pieces[side]]
+        return remote(slot, slot, h_send.at[send, side], h_recv.at[source, side], fs_id, tp)
 
     def dir_store(source):
         send_out(dir_ref.at[source], dir_out.at[source], dir_sem.at[source])
 
-    for i in range(1, outer):
-        start(dir_copy(me, i - 1, level(i) * PAIR + x))
-    start(dir_copy(me, outer - 1, mate))
+    moments = ((fq, sq), (fk, sk))
+    for side, cols in enumerate(pieces):
+        first, second = moments[side]
+        dir_ref[me, :, cols] = moment_update(scaled[:, cols], first[...], second[...])[2]
+        for i in range(1, outer):
+            start(dir_copy(me, i - 1, level(i) * PAIR + x, side))
+        start(dir_copy(me, outer - 1, mate, side))
     send_out(scaled_ref, scaled_out, out_sem.at[1])
     dir_store(me)
     for i in range(outer):
         source = level(i) * PAIR + (1 - x)
         master_copy(source, 0, mate).wait_recv()
     send_out(master_ref, master_out, out_sem.at[2])
-    for i in range(1, outer):
-        source = level(i) * PAIR + x
-        copy = dir_copy(source, outer - 1 + i, mate)
-        copy.wait_recv()
-        start(copy)
-        dir_store(source)
+    for side in range(len(pieces)):
+        for i in range(1, outer):
+            source = level(outer - i) * PAIR + x
+            copy = dir_copy(source, outer - 1 + i, mate, side)
+            copy.wait_recv()
+            start(copy)
+            if side == len(pieces) - 1:
+                dir_store(source)
     for i in range(outer):
-        source = level(i) * PAIR + (1 - x)
-        dir_copy(source, 0, mate).wait_recv()
+        source = level(outer - i) * PAIR + (1 - x)
+        for side in range(len(pieces)):
+            dir_copy(source, 0, mate, side).wait_recv()
         dir_store(source)
     for copy, when in pending:
         if when is None:
@@ -463,12 +487,12 @@
             dma((n,)),
             dma((4 * outer - 3,)),
             dma((n,)),
-            dma((2 * outer - 1,)),
-            dma((n,)),
-            dma((outer,)),
-            dma((outer,)),
-            dma((outer,)),
-            dma((outer,)),
+            dma((2 * outer - 1, 2)),
+            dma((n, 2)),
+            dma((outer, 2)),
+            dma((outer, 2)),
+            dma((outer, 2)),
+            dma((outer, 2)),
             dma((tp_size,)),
             dma((tp_size,)),
             dma((n,)),

time: 56.6 us -> 54.2 us (0.958)
  Pallas kernels: 55.8 us -> 53.4 us
    pallas_call x1, Pallas kernels: 52.3 us -> 49.9 us  [kernel_body(): pl.pallas_call(functools.partial(exchange_kernel, n, tp_size), out_shape=...]
where the time goes in v3:
time: 54.2 us; the launch traced here: 54 us
  Pallas kernels  53.4 us (99%)
  between operations  0.64 us (1%)
    pallas_call x1, Pallas kernels, kernel_body(): pl.pallas_call(functools.partial(exchange_kernel, n, tp_size), out_shape=...  49.9 us
    pallas_call x1, Pallas kernels, kernel_body(): pl.pallas_call(apply_kernel, out_shape=shapes, in_specs=[vmem] * 10, out_...  3.53 us

profile of v3, /device:TPU:0, one launch (start us, length us, event | category | flops | bytes accessed | tf_op | source)
XLA Modules:
  0.0 54.0 jit_solution(16358270812035738137)
XLA Ops:
  0.6 49.9 %exchange.1 = (f32[32,1280]{1,0:T(8,128)}, bf16[8,32,1280]{2,1,0:T(8,128)(2,1)}, bf16[8,64,1280]{2,1,0:T(8,128)(2,1)}, bf16[8,2,64,256]{3,2,1,0:T(8,128)(2,1)}) custom-call(bf16[768,512]{1,0:T(8,128)(2,1)} %lq_hbm.1, bf16[768,768]{1,0:T(8,128)(2,1)} %gq_hbm.1, bf16[768,512]{1,0:T(8,128)(2,1)} %lk_hbm.1, bf16[768,512]{1,0:T(8,128)(2,1)} %gk_hbm.1, ...), custom_call_target="tpu_custom_call" | custom-call | tf_op jit(solution)/shard_map/exchange/pallas_call | solution.py:445
  50.5 3.5 %apply.1 = (f32[32,768]{1,0:T(8,128)}, f32[32,768]{1,0:T(8,128)}, f32[64,768]{1,0:T(8,128)}, bf16[512,768]{1,0:T(8,128)(2,1)}, f32[32,512]{1,0:T(8,128)}, /*inde...) custom-call(f32[32,1280]{1,0:T(8,128)} %get-tuple-element.12.scaled_ref, ...), custom_call_target="tpu_custom_call" | custom-call | tf_op jit(solution)/shard_map/apply/pallas_call | solution.py:517
